TPU v7x, 32 devices: a whole 2x2x4 slice. The times are simulated.
32 devices in a mesh: fs: 8 (over z, y), tp: 4 (over x, core).
Axes of the slice: x: 2, y: 2, z: 4, core: 2. Of those that a mesh axis runs over, the one named last changes fastest.
Arguments:
- latent_in: bfloat16 [24576, 512], P('fs'), may hold values from -6 to 6
- query_cot: bfloat16 [24576, 1536], P('fs', 'tp'), may hold values from -6 to 6
- attn_out: bfloat16 [24576, 1024], P('fs'), may hold values from -6 to 6
- mix_cot: bfloat16 [24576, 2048], P('fs', 'tp'), may hold values from -6 to 6
- query_weight: float32 [512, 1536], P('fs', 'tp'), may hold values from -0.25 to 0.25
- output_weight: float32 [1024, 2048], P('fs', 'tp'), may hold values from -0.1875 to 0.1875
- query_factor: bfloat16 [512, 256], P('fs'), may hold values from -0.25 to 0.25
- output_factor: bfloat16 [1024, 256], P('fs'), may hold values from -0.1875 to 0.1875
- query_mean: float32 [256, 1536], P('fs', 'tp'), may hold values from -3 to 3
- query_square: float32 [256, 1536], P('fs', 'tp'), may hold values from 0.05 to 1
- output_mean: float32 [256, 2048], P('fs', 'tp'), may hold values from -3 to 3
- output_square: float32 [256, 2048], P('fs', 'tp'), may hold values from 0.05 to 1
Outputs:
- step_query: float32 [512, 1536], P('fs', 'tp')
- step_output: float32 [1024, 2048], P('fs', 'tp')
- new_query: float32 [512, 1536], P('fs', 'tp')
- new_output: float32 [1024, 2048], P('fs', 'tp')
- copy_query: bfloat16 [512, 1536], P(None, 'tp')
- copy_output: bfloat16 [1024, 2048], P(None, 'tp')
- query_mean_new: float32 [256, 1536], P('fs', 'tp')
- query_square_new: float32 [256, 1536], P('fs', 'tp')
- output_mean_new: float32 [256, 2048], P('fs', 'tp')
- output_square_new: float32 [256, 2048], P('fs', 'tp')
All inputs are finite; a program needn't handle non-finite values.
Results may differ from a plain program's by a relative error of at most 0.0085.
Values may be sent and summed in bfloat16 or wider, within the bound.
A program may use at most 64 MiB of HBM per device.

v0:
```python
import math

import jax
import jax.numpy as jnp
from jax import lax
from jax.sharding import PartitionSpec as P


def over_rows_exact(left, right):
    return lax.dot_general(
        left,
        right,
        (((0,), (0,)), ((), ())),
        precision=lax.Precision.HIGHEST,
        preferred_element_type=jnp.float32,
    )


def exact_dot(left, right):
    return jnp.dot(left, right, precision=lax.Precision.HIGHEST, preferred_element_type=jnp.float32)


def moments(mean, square, low):
    mean_new = 0.8 * mean + 0.2 * low
    square_new = 0.9 * square + 0.1 * low * low
    return (mean_new, square_new, mean_new / jnp.sqrt(square_new))


def on_device(
    latent_in,
    query_cot,
    attn_out,
    mix_cot,
    query_weight,
    output_weight,
    query_factor,
    output_factor,
    query_mean,
    query_square,
    output_mean,
    output_square,
):
    tokens_local = latent_in.shape[0]
    inv_root = 1.0 / math.sqrt(tokens_local * lax.axis_size("fs"))
    weight_rows = query_weight.shape[0]
    query_width = query_weight.shape[1]
    output_width = output_weight.shape[1]
    rank = query_factor.shape[1]
    factor_query = query_factor.astype(jnp.float32)
    factor_output = output_factor.astype(jnp.float32)
    stacked = jnp.concatenate([query_factor, output_factor.reshape(weight_rows, 2 * rank)], axis=1)
    piece = lax.all_gather(stacked, "fs", axis=0, tiled=True)
    count = piece.shape[0]
    piece_query = piece[:, :rank]
    piece_output = piece[:, rank:].reshape(2 * count, rank)
    latent_low = jnp.dot(latent_in, piece_query, preferred_element_type=jnp.float32)
    output_low = jnp.dot(attn_out, piece_output, preferred_element_type=jnp.float32)
    cot_query = query_cot.astype(jnp.float32)
    cot_output = mix_cot.astype(jnp.float32)
    low = lax.psum_scatter(
        jnp.concatenate(
            [over_rows_exact(latent_low, cot_query), over_rows_exact(output_low, cot_output)],
            axis=1,
        )
        * inv_root,
        "fs",
        scatter_dimension=0,
        tiled=True,
    )
    mean_q, square_q, direction_q = moments(query_mean, query_square, low[:, :query_width])
    mean_o, square_o, direction_o = moments(output_mean, output_square, low[:, query_width:])
    joined = jnp.concatenate([direction_q, direction_o], axis=1)
    piece = lax.all_gather(joined, "fs", axis=0, tiled=True)
    piece_query = piece[:, :query_width]
    piece_output = piece[:, query_width:]
    product_q = exact_dot(factor_query, piece_query)
    product_o = exact_dot(factor_output, piece_output)
    square_sum_q = jnp.sum(piece_query * piece_query)
    square_sum_o = jnp.sum(piece_output * piece_output)
    square_sum_q, square_sum_o = lax.psum((square_sum_q, square_sum_o), "tp")
    columns = lax.axis_size("tp")
    scale_q = 1.0 / jnp.sqrt(square_sum_q / (rank * query_width * columns) + 0.25)
    scale_o = 1.0 / jnp.sqrt(square_sum_o / (rank * output_width * columns) + 0.25)
    step_q = product_q * scale_q
    step_o = product_o * scale_o
    new_q = query_weight - 0.02 * step_q
    new_o = output_weight - 0.02 * step_o
    copy_q, copy_o = (
        lax.all_gather(new_q.astype(jnp.bfloat16), "fs", axis=0, tiled=True),
        lax.all_gather(new_o.astype(jnp.bfloat16), "fs", axis=0, tiled=True),
    )
    return (step_q, step_o, new_q, new_o, copy_q, copy_o, mean_q, square_q, mean_o, square_o)


def solution(mesh):
    placed = (
        P("fs", None),
        P("fs", "tp"),
        P("fs", None),
        P("fs", "tp"),
        P("fs", "tp"),
        P("fs", "tp"),
        P("fs", None),
        P("fs", None),
        P("fs", "tp"),
        P("fs", "tp"),
        P("fs", "tp"),
        P("fs", "tp"),
    )
    return jax.shard_map(
        on_device,
        mesh=mesh,
        in_specs=placed,
        out_specs=(
            P("fs", "tp"),
            P("fs", "tp"),
            P("fs", "tp"),
            P("fs", "tp"),
            P(None, "tp"),
            P(None, "tp"),
            P("fs", "tp"),
            P("fs", "tp"),
            P("fs", "tp"),
            P("fs", "tp"),
        ),
        check_vma=False,
    )
```

profile of v0, /device:TPU:0, one launch (start us, length us, event | category | flops | bytes accessed | tf_op | source)
XLA Modules:
  0.0 222.5 jit_solution(15410756157516759799)
XLA Ops:
  7.2 0.0 reduce-scatter.2.cloned.1.call-start
  7.2 1.0 reshape.26
  8.3 0.8 pad_maximum_fusion.1
  9.0 33.9 %all_gather.12 = bf16[512,768]{1,0:T(8,128)(2,1)S(1)} all-gather(bf16[64,768]{1,0:T(8,128)(2,1)S(1)} %pad_maximum_fusion.1), channel_id=1, replica_groups=mesh['fs'=8,'tp'=4] {'fs'}, dimensions={0}, use_global_device_ids=true | all-gather | bytes 884736 | tf_op jit(solution)/shard_map/all_gather | solution.py:52
  42.9 0.9 copy-done.2
  43.8 0.8 slice.25
  44.6 2.0 reshape.27
  46.6 2.0 fusion.4
  48.7 4.9 %fusion.13 = f32[256,3072]{1,0:T(8,128)S(1)} fusion(bf16[1024,256]{1,0:T(8,128)(2,1)S(1)} %copy-done.5, bf16[3072,1024]{1,0:T(8,128)(2,1)} %param.14), kind=kOutput, calls=%fused_computation.26 | convolution fusion | flops 1610612736 | bytes 9961472 | tf_op jit(solution)/shard_map/dot_general | solution.py:57
  53.6 2.6 %fusion.14 = f32[256,512]{1,0:T(8,128)S(1)} fusion(f32[256,3072]{1,0:T(8,128)S(1)} %fusion.13, bf16[3072,512]{1,0:T(8,128)(2,1)S(1)} %copy-done.3), kind=kOutput, calls=%fused_computation.27 | convolution fusion | flops 4831838208 | bytes 6815744 | tf_op jit(solution)/shard_map/dot_general | solution.py:10
  56.2 2.6 %fusion.12 = f32[256,384]{1,0:T(8,128)S(1)} fusion(f32[256,3072]{1,0:T(8,128)S(1)} %fusion.4, bf16[3072,384]{1,0:T(8,128)(2,1)S(1)} %copy-done.4), kind=kOutput, calls=%fused_computation.25 | convolution fusion | flops 3623878656 | bytes 5898240 | tf_op jit(solution)/shard_map/dot_general | solution.py:10
  58.9 1.0 maximum_multiply_fusion
  59.9 0.0 reduce-scatter.2.cloned.1.call-update
  59.9 0.0 all-gather.2.cloned.1.call-start
  60.0 64.6 %reduce-scatter.2.cloned.1.call-done = f32[32,896]{1,0:T(8,128)} async-done(((f32[256,896]{1,0:T(8,128)}), f32[32,896]{1,0:T(8,128)}) %reduce-scatter.2.cloned.1.call-update) | async-done | bytes 114704 | tf_op jit(solution)/shard_map/reduce_scatter | solution.py:60
  124.6 1.5 rsqrt_multiply_fusion
  126.1 1.5 rsqrt_multiply_fusion.1
  127.6 32.5 %all_gather.13 = f32[256,896]{1,0:T(8,128)S(1)} all-gather(f32[32,896]{1,0:T(8,128)S(1)} %pad_maximum_fusion), channel_id=1, replica_groups=mesh['fs'=8,'tp'=4] {'fs'}, dimensions={0}, use_global_device_ids=true | all-gather | bytes 1032192 | tf_op jit(solution)/shard_map/all_gather | solution.py:73
  160.1 0.8 multiply_reduce_fusion
  160.9 0.1 copy-done.1
  161.0 0.7 multiply_reduce_fusion.1
  161.7 1.1 copy.22
  162.8 6.3 %all-reduce = (f32[]{:T(128)}, f32[]{:T(128)}) all-reduce(f32[]{:T(128)} %multiply_reduce_fusion.1, f32[]{:T(128)} %multiply_reduce_fusion), channel_id=1, replica_groups=mesh['fs'=8,'tp'=4] {'tp'}, use_global_device_ids=true, to_apply=%region_2.0 | all-reduce | flops 2 | bytes 16 | tf_op jit(solution)/shard_map/psum | solution.py:80
  169.8 2.5 %fusion.8 = (bf16[128,512]{0,1:T(8,128)(2,1)}, f32[128,512]{0,1:T(8,128)}, f32[128,512]{0,1:T(8,128)}) fusion(f32[128,512]{0,1:T(8,128)S(1)} %copy.22, f32[]{:T(128)S(6)} %sqrt.15, bf16[128,256]{1,0:T(8,128)(2,1)S(1)} %copy-done.6, f32[256,896]{1,0:T(8,128)} %copy-done.1), kind=kOutput, calls=%fused_computation.23 | convolution fusion | flops 201588736 | bytes 1507332 | tf_op jit(solution)/shard_map/dot_general | solution.py:20
  172.3 0.0 all-gather.2.cloned.1.call-update
  172.3 1.8 copy.23
  174.1 1.8 copy.24
  176.6 2.0 fusion.9
  178.5 31.5 %all_gather.14 = bf16[512,384]{1,0:T(8,128)(2,1)S(1)} all-gather(bf16[64,384]{1,0:T(8,128)(2,1)S(1)} %get-tuple-element.24), channel_id=1, replica_groups=mesh['fs'=8,'tp'=4] {'fs'}, dimensions={0}, use_global_device_ids=true | all-gather | bytes 442368 | tf_op jit(solution)/shard_map/all_gather | solution.py:89
  210.0 2.6 %all-gather.2.cloned.1.call-done = bf16[1024,512]{0,1:T(8,128)(2,1)} async-done(((bf16[128,512]{0,1:T(8,128)(2,1)}), bf16[1024,512]{0,1:T(8,128)(2,1)}) %all-gather.2.cloned.1.call-update) | async-done | bytes 1048592 | tf_op jit(solution)/shard_map/all_gather | solution.py:90
  212.7 2.3 %copy.25 = bf16[1024,512]{1,0:T(8,128)(2,1)} copy(bf16[1024,512]{0,1:T(8,128)(2,1)} %all-gather.2.cloned.1.call-done) | data formatting | bytes 2097152
  215.0 0.7 copy.27
  (23 shorter events, 0.1 us)
Async XLA Ops:
  7.2 39.4 %copy-start = (bf16[3072,512]{1,0:T(8,128)(2,1)S(1)}, bf16[3072,512]{1,0:T(8,128)(2,1)}, u32[]{:S(2)}) copy-start(bf16[3072,512]{1,0:T(8,128)(2,1)} %param.12) | copy-start | bytes 9437188
  7.2 117.4 %reduce-scatter.2.cloned.1.call-start = ((), (), s32[]{:S(2)}) async-start(), calls=%async_computation.1 | async-start | bytes 1032192 | tf_op jit(solution)/shard_map/reduce_scatter | solution.py:60
  42.9 0.9 copy-start.2
  46.6 2.1 copy-start.5
  48.7 4.9 %copy-start.3 = (bf16[3072,512]{1,0:T(8,128)(2,1)S(1)}, bf16[3072,512]{1,0:T(8,128)(2,1)}, u32[]{:S(2)}) copy-start(bf16[3072,512]{1,0:T(8,128)(2,1)} %param.15) | copy-start | bytes 9437188
  53.5 2.6 %copy-start.4 = (bf16[3072,384]{1,0:T(8,128)(2,1)S(1)}, bf16[3072,384]{1,0:T(8,128)(2,1)}, u32[]{:S(2)}) copy-start(bf16[3072,384]{1,0:T(8,128)(2,1)} %param.13) | copy-start | bytes 7077892
  56.2 68.4 %copy-start.8 = (f32[32,512]{1,0:T(8,128)S(1)}, f32[32,512]{1,0:T(8,128)}, u32[]{:S(2)}) copy-start(f32[32,512]{1,0:T(8,128)} %param.23) | copy-start | bytes 196612
  56.2 68.4 %copy-start.9 = (f32[32,512]{1,0:T(8,128)S(1)}, f32[32,512]{1,0:T(8,128)}, u32[]{:S(2)}) copy-start(f32[32,512]{1,0:T(8,128)} %param.22) | copy-start | bytes 196612
  56.2 69.9 %copy-start.10 = (f32[32,384]{1,0:T(8,128)S(1)}, f32[32,384]{1,0:T(8,128)}, u32[]{:S(2)}) copy-start(f32[32,384]{1,0:T(8,128)} %param.21) | copy-start | bytes 147460
  56.2 69.9 %copy-start.11 = (f32[32,384]{1,0:T(8,128)S(1)}, f32[32,384]{1,0:T(8,128)}, u32[]{:S(2)}) copy-start(f32[32,384]{1,0:T(8,128)} %param.20) | copy-start | bytes 147460
  58.9 110.9 %copy-start.6 = (bf16[128,256]{1,0:T(8,128)(2,1)S(1)}, bf16[128,256]{1,0:T(8,128)(2,1)}, u32[]{:S(2)}) copy-start(bf16[128,256]{1,0:T(8,128)(2,1)} %param.19) | copy-start | bytes 196612
  59.9 116.6 %copy-start.7 = (bf16[64,256]{1,0:T(8,128)(2,1)S(1)}, bf16[64,256]{1,0:T(8,128)(2,1)}, u32[]{:S(2)}) copy-start(bf16[64,256]{1,0:T(8,128)(2,1)} %param.18) | copy-start | bytes 98308
  59.9 152.8 %all-gather.2.cloned.1.call-start = ((), (), s32[]{:S(2)}) async-start(), calls=%async_computation.2 | async-start | bytes 1179648 | tf_op jit(solution)/shard_map/all_gather | solution.py:90
  160.1 0.9 copy-start.1
Sparse Core Ops, SparseCore 0:
  60.0 64.5 reduce-scatter.1
  172.4 40.2 all-gather.1
where the time goes:
time: 223 us
  blocking collectives  104 us (47%)
  waiting for transfers between devices  67.3 us (30%)
  matrix products  16.6 us (7%)
  between operations  15.6 us (7%)
  local copies, waits for them, and re-layouts  12.6 us (6%)
  other arithmetic  6.25 us (3%)
    reduce_scatter x1, waiting for transfers between devices, on_device(): lax.psum_scatter(jnp.concatenate([over_rows_exact(latent_low, cot_query),...  64.6 us
    all_gather x1, blocking collectives, on_device(): piece = lax.all_gather(stacked, 'fs', axis=0, tiled=True)  33.9 us
    all_gather x1, blocking collectives, on_device(): piece = lax.all_gather(joined, 'fs', axis=0, tiled=True)  32.5 us
    all_gather x1, blocking collectives, on_device(): lax.all_gather(new_q.astype(jnp.bfloat16), 'fs', axis=0, tiled=True)  31.5 us
    unnamed x29, local copies, waits for them, and re-layouts  8.72 us
    psum x1, blocking collectives, on_device(): square_sum_q, square_sum_o = lax.psum((square_sum_q, square_sum_o), 'tp')  6.31 us
    dot_general x2, matrix products, over_rows_exact(): lax.dot_general(left, right, (((0,), (0,)), ((), ())), precision=lax.Prec...  5.23 us
    dot_general x1, matrix products, on_device(): jnp.dot(attn_out, piece_output, preferred_element_type=jnp.float32)  4.85 us
  transfers between devices with their start and end apart: 2, of which 2 were waited for; matrix products, arithmetic and copies ran while one was open for 2% of the time, Pallas kernels for 0%

commit v1 on v0

v1 whole, which is shorter than its diff:
```python
import functools
import math

import jax
import jax.numpy as jnp
from jax import lax
from jax.experimental import pallas as pl
from jax.experimental.pallas import tpu as pltpu
from jax.sharding import PartitionSpec as P

MESH = pl.DeviceIdType.MESH
BF16 = jnp.bfloat16
F32 = jnp.float32
CHUNKS = 4


def grid_of(count):
    inner = max(d for d in range(1, count + 1) if count % d == 0 and d * d <= count)
    return count // inner, inner


def copies_of(nz, ny, nt):
    n = nz * ny
    per_gather = (nz - 1) + nz * (ny - 1)
    return per_gather + ny + 4 * per_gather + 2 * (nz + ny - 2) + (nt - 1) + (n - 1)


def over_rows(left, right):
    return lax.dot_general(left, right, (((0,), (0,)), ((), ())), preferred_element_type=F32)


def fused_kernel(
    nz, ny, nt, inv_root,
    latent_hbm, cot_hbm, attn_hbm, mix_hbm,
    wq_ref, wo_ref, fq_hbm, fo_hbm, qm_ref, qs_ref, om_ref, os_ref,
    fac, wq_all, wo_all, dq_all, do_all, low_q, low_o, total,
    latent, cot, attn, mix, grad_q, grad_o,
    part_q, part_o, yin_q, yin_o, acc_q, acc_o, zout_q, zout_o, zin_q, zin_o,
    tile_tp, tile_fs,
    load_sem, fac_sem, send_sem, recv_sem,
):
    n = nz * ny
    f = lax.axis_index("fs")
    t = lax.axis_index("tp")
    z, y = f // ny, f % ny
    half_cols = fac.shape[-1] // 2
    half = pl.ds(pl.multiple_of((t % 2) * half_cols, half_cols), half_cols)
    twin = t + 1 - 2 * (t % 2)
    rq = fq_hbm.shape[0]
    tokens = latent_hbm.shape[0]
    step = tokens // CHUNKS

    def load(k, pair, sem):
        rows = pl.ds(pl.multiple_of(k * step, step), step)
        return [
            pltpu.make_async_copy(src.at[rows, :], dst.at[rows, :], load_sem.at[k, sem + i])
            for i, (src, dst) in enumerate(pair)
        ]

    pair_o = ((attn_hbm, attn), (mix_hbm, mix))
    pair_q = ((latent_hbm, latent), (cot_hbm, cot))
    own = [
        pltpu.make_async_copy(fq_hbm.at[:, half], fac.at[z, y, pl.ds(0, rq), half], fac_sem.at[0]),
        pltpu.make_async_copy(
            fo_hbm.at[:, half], fac.at[z, y, pl.ds(rq, fo_hbm.shape[0]), half], fac_sem.at[1]
        ),
    ]
    for c in own:
        c.start()
    for k in range(CHUNKS):
        for c in load(k, pair_o, 0):
            c.start()
    for k in range(CHUNKS):
        for c in load(k, pair_q, 2):
            c.start()

    barrier = pltpu.get_barrier_semaphore()
    for d in range(1, n):
        pl.semaphore_signal(barrier, inc=1, device_id={"fs": (f + d) % n}, device_id_type=MESH)
    for d in range(1, nt):
        pl.semaphore_signal(barrier, inc=1, device_id={"tp": (t + d) % nt}, device_id_type=MESH)

    wq_all[z, y] = wq_ref[...].astype(BF16)
    wo_all[z, y] = wo_ref[...].astype(BF16)
    for c in own:
        c.wait()
    pl.semaphore_wait(barrier, n - 1 + nt - 1)

    started = []

    def send(src, dst, device):
        k = len(started)
        c = pltpu.make_async_remote_copy(
            src_ref=src, dst_ref=dst, send_sem=send_sem.at[k], recv_sem=recv_sem.at[k],
            device_id=device, device_id_type=MESH,
        )
        c.start()
        started.append(c)
        return c

    def to_z(d):
        return {"fs": ((z + d) % nz) * ny + y}

    def to_y(d):
        return {"fs": z * ny + (y + d) % ny}

    def z_send(block, ds):
        return {d: send(block(z), block(z), to_z(d)) for d in ds}

    def y_send(block, back):
        zz = (z + nz - back) % nz
        return [send(block(zz), block(zz), to_y(d)) for d in range(1, ny)]

    fac_block = lambda zz: fac.at[zz, y, :, half]
    wq_block = lambda zz: wq_all.at[zz, y]
    wo_block = lambda zz: wo_all.at[zz, y]
    dq_block = lambda zz: dq_all.at[zz, y]
    do_block = lambda zz: do_all.at[zz, y]

    far = range(1, nz)
    fac_z = z_send(fac_block, far)
    fac_y = y_send(fac_block, 0)
    early = far[: max(1, len(far) - 1)]
    w_z = {}
    for d in early:
        w_z[d] = (send(wo_block(z), wo_block(z), to_z(d)), send(wq_block(z), wq_block(z), to_z(d)))

    grad_o[...] = jnp.zeros_like(grad_o)
    grad_q[...] = jnp.zeros_like(grad_q)

    def product(k, pair, sem, out):
        for c in load(k, pair, sem):
            c.wait()
        rows = pl.ds(pl.multiple_of(k * step, step), step)
        out[...] += over_rows(pair[1][1][rows, :], pair[0][1][rows, :])

    @pl.loop(0, CHUNKS // 2)
    def _(k):
        product(k, pair_o, 0, grad_o)

    for d in far:
        fac_z[d].wait_recv()
        fac_y += y_send(fac_block, d)
    swap = [send(fac.at[:, y, :, half], fac.at[:, y, :, half], {"tp": twin})]

    @pl.loop(CHUNKS // 2, CHUNKS)
    def _(k):
        product(k, pair_o, 0, grad_o)

    for c in fac_y:
        c.wait_recv()
    for d in range(1, ny):
        other = fac.at[:, (y + ny - d) % ny, :, half]
        swap.append(send(other, other, {"tp": twin}))

    @pl.loop(0, CHUNKS)
    def _(k):
        product(k, pair_q, 2, grad_q)

    for c in swap:
        c.wait_recv()

    rank = fac.shape[-1]
    block = rank // n

    def project(lo, hi, grad, part):
        factor = fac[:, :, lo:hi, :].reshape(n * (hi - lo), rank)
        g = grad[...]
        top = g.astype(BF16)
        rest = (g - top.astype(F32)).astype(BF16)
        dims = (((0,), (1,)), ((), ()))
        low = lax.dot_general(factor, top, dims, preferred_element_type=F32)
        low += lax.dot_general(factor, rest, dims, preferred_element_type=F32)
        low *= inv_root
        for i in range(nz):
            for j in range(ny):
                at = (i * ny + j) * block
                part[i, j] = low[at:at + block, :]

    matrices = (
        (rq, fac.shape[2], grad_o, part_o, yin_o, acc_o, zout_o, zin_o),
        (0, rq, grad_q, part_q, yin_q, acc_q, zout_q, zin_q),
    )
    y_in = []
    for lo, hi, grad, part, yin, acc, zout, zin in matrices:
        project(lo, hi, grad, part)
        copies = []
        for d in range(1, ny):
            yy = (y + d) % ny
            acc_send = yin.at[d - 1]
            for i in range(nz):
                yin[ny - 1 + d - 1, i] = part[i, yy].astype(BF16)
            copies.append(send(yin.at[ny - 1 + d - 1], acc_send, to_y(d)))
        y_in.append(copies)

    z_in = []
    for (lo, hi, grad, part, yin, acc, zout, zin), copies in zip(matrices, y_in):
        for i in range(nz):
            acc[i] = part[i, y]
        for d, c in enumerate(copies):
            c.wait_recv()
            for i in range(nz):
                acc[i] += yin[d, i].astype(F32)
        copies = []
        for d in far:
            zout[d - 1] = acc[(z + d) % nz].astype(BF16)
            copies.append(send(zout.at[d - 1], zin.at[d - 1], to_z(d)))
        z_in.append(copies)

    for d in far:
        if d not in w_z:
            w_z[d] = (send(wo_block(z), wo_block(z), to_z(d)), send(wq_block(z), wq_block(z), to_z(d)))
    w_y = y_send(wo_block, 0) + y_send(wq_block, 0)

    def forward_weights(d):
        w_z[d][0].wait_recv()
        w_z[d][1].wait_recv()
        return y_send(wo_block, d) + y_send(wq_block, d)

    w_y += forward_weights(1) if nz > 1 else []

    sides = (
        (matrices[0], z_in[0], om_ref, os_ref, low_o, do_all, 1),
        (matrices[1], z_in[1], qm_ref, qs_ref, low_q, dq_all, 0),
    )
    d_z = []
    d_y = []
    for (_, _, _, _, _, acc, _, zin), copies, mean_ref, square_ref, low_ref, d_all, slot in sides:
        low = acc[z]
        for d, c in zip(far, copies):
            c.wait_recv()
            low += zin[d - 1].astype(F32)
        low_ref[...] = low
        mean_new = 0.8 * mean_ref[...] + 0.2 * low
        square_new = 0.9 * square_ref[...] + 0.1 * low * low
        direction = mean_new / jnp.sqrt(square_new)
        d_all[z, y] = direction.astype(BF16)
        tile_tp[0, slot] = jnp.broadcast_to(jnp.sum(direction * direction), tile_tp.shape[2:])
        where = lambda zz, d_all=d_all: d_all.at[zz, y]
        d_z.append((where, z_send(where, far)))
        d_y += y_send(where, 0)

    tiles = [
        send(tile_tp.at[0], tile_tp.at[d], {"tp": (t + d) % nt}) for d in range(1, nt)
    ]
    for c in tiles:
        c.wait_recv()
    tile_fs[0] = jnp.sum(tile_tp[...], axis=0)
    tiles = [
        send(tile_fs.at[0], tile_fs.at[d], {"fs": (f + d) % n}) for d in range(1, n)
    ]
    for d in far:
        for where, copies in d_z:
            copies[d].wait_recv()
            d_y += y_send(where, d)
    for d in far[1:]:
        w_y += forward_weights(d)
    for c in tiles:
        c.wait_recv()
    total[...] = jnp.sum(tile_fs[...], axis=0)
    for c in d_y + w_y:
        c.wait_recv()
    for c in started:
        c.wait_send()


def on_device(
    nz, ny, nt,
    latent_in, query_cot, attn_out, mix_cot, query_weight, output_weight,
    query_factor, output_factor, query_mean, query_square, output_mean, output_square,
):
    n = nz * ny
    tokens = latent_in.shape[0]
    inv_root = 1.0 / math.sqrt(tokens * n)
    rq, cq = query_weight.shape
    ro, co = output_weight.shape
    rank = query_factor.shape[1]
    block = rank // n
    vmem = pl.BlockSpec(memory_space=pltpu.VMEM)
    hbm = pl.BlockSpec(memory_space=pl.ANY)
    copies = copies_of(nz, ny, nt)
    fac, wq, wo, dq, do, low_q, low_o, total = pl.pallas_call(
        functools.partial(fused_kernel, nz, ny, nt, inv_root),
        name="moment_exchange",
        in_specs=[hbm] * 4 + [vmem] * 2 + [hbm] * 2 + [vmem] * 4,
        out_specs=[vmem] * 8,
        out_shape=[
            jax.ShapeDtypeStruct((nz, ny, rq + ro, rank), BF16),
            jax.ShapeDtypeStruct((nz, ny, rq, cq), BF16),
            jax.ShapeDtypeStruct((nz, ny, ro, co), BF16),
            jax.ShapeDtypeStruct((nz, ny, block, cq), BF16),
            jax.ShapeDtypeStruct((nz, ny, block, co), BF16),
            jax.ShapeDtypeStruct((block, cq), F32),
            jax.ShapeDtypeStruct((block, co), F32),
            jax.ShapeDtypeStruct((2, 8, 128), F32),
        ],
        scratch_shapes=[
            pltpu.VMEM(latent_in.shape, BF16),
            pltpu.VMEM(query_cot.shape, BF16),
            pltpu.VMEM(attn_out.shape, BF16),
            pltpu.VMEM(mix_cot.shape, BF16),
            pltpu.VMEM((cq, n * rq), F32),
            pltpu.VMEM((co, n * ro), F32),
            pltpu.VMEM((nz, ny, block, cq), F32),
            pltpu.VMEM((nz, ny, block, co), F32),
            pltpu.VMEM((2 * max(ny - 1, 1), nz, block, cq), BF16),
            pltpu.VMEM((2 * max(ny - 1, 1), nz, block, co), BF16),
            pltpu.VMEM((nz, block, cq), F32),
            pltpu.VMEM((nz, block, co), F32),
            pltpu.VMEM((max(nz - 1, 1), block, cq), BF16),
            pltpu.VMEM((max(nz - 1, 1), block, co), BF16),
            pltpu.VMEM((max(nz - 1, 1), block, cq), BF16),
            pltpu.VMEM((max(nz - 1, 1), block, co), BF16),
            pltpu.VMEM((nt, 2, 8, 128), F32),
            pltpu.VMEM((n, 2, 8, 128), F32),
            pltpu.SemaphoreType.DMA((CHUNKS, 4)),
            pltpu.SemaphoreType.DMA((2,)),
            pltpu.SemaphoreType.DMA((copies,)),
            pltpu.SemaphoreType.DMA((copies,)),
        ],
        compiler_params=pltpu.CompilerParams(
            collective_id=0, has_side_effects=True, vmem_limit_bytes=60 * 1024 * 1024
        ),
    )(
        latent_in, query_cot, attn_out, mix_cot, query_weight, output_weight,
        query_factor, output_factor, query_mean, query_square, output_mean, output_square,
    )

    def finish(factor, factor_all, direction, weight, weight_all, mean, square, low, slot):
        mean_new = 0.8 * mean + 0.2 * low
        square_new = 0.9 * square + 0.1 * low * low
        cols = weight.shape[1]
        scale = 1.0 / jnp.sqrt(total[slot, 0, 0] / (rank * cols * nt) + 0.25)
        direction = direction.reshape(rank, cols)
        step = jnp.dot(factor, direction, preferred_element_type=F32) * scale
        new = weight - 0.02 * step
        full = jnp.dot(factor_all.reshape(-1, rank), direction, preferred_element_type=F32) * scale
        copy = (weight_all.reshape(-1, cols).astype(F32) - 0.02 * full).astype(BF16)
        return step, new, copy, mean_new, square_new

    step_q, new_q, copy_q, mean_q, square_q = finish(
        query_factor, fac[:, :, :rq], dq, query_weight, wq, query_mean, query_square, low_q, 0
    )
    step_o, new_o, copy_o, mean_o, square_o = finish(
        output_factor, fac[:, :, rq:], do, output_weight, wo, output_mean, output_square, low_o, 1
    )
    return (step_q, step_o, new_q, new_o, copy_q, copy_o, mean_q, square_q, mean_o, square_o)


def solution(mesh):
    nz, ny = grid_of(mesh.shape["fs"])
    rows, both, cols = P("fs", None), P("fs", "tp"), P(None, "tp")
    return jax.shard_map(
        functools.partial(on_device, nz, ny, mesh.shape["tp"]),
        mesh=mesh,
        in_specs=(rows, both, rows, both, both, both, rows, rows, both, both, both, both),
        out_specs=(both, both, both, both, cols, cols, both, both, both, both),
        check_vma=False,
    )
```

time: 223 us -> 71.8 us (0.32)
  blocking collectives: 104 us -> 0 us
  waiting for transfers between devices: 67.3 us -> 0 us
  Pallas kernels: 0 us -> 59.4 us
  between operations: 15.6 us -> 2.23 us
  matrix products: 16.6 us -> 5.47 us
  local copies, waits for them, and re-layouts: 12.6 us -> 3.22 us
  other arithmetic: 6.25 us -> 1.33 us
    all_gather x3 -> x0, blocking collectives: 97.9 us -> none  [the longest x1 33.9 us: on_device(): piece = lax.all_gather(stacked, 'fs', axis=0, tiled=True)]
    reduce_scatter x1 -> x0, waiting for transfers between devices: 64.6 us -> none  [on_device(): lax.psum_scatter(jnp.concatenate([over_rows_exact(latent_low, cot_query),...]
    pallas_call x0 -> x1, Pallas kernels: none -> 59.4 us  [on_device(): pl.pallas_call(functools.partial(fused_kernel, nz, ny, nt, inv_root), nam...]
    dot_general x6 -> x4, matrix products: 16.6 us -> 5.47 us  [the longest x2 2.99 us: finish(): step = jnp.dot(factor, direction, preferred_element_type=F32) * scale]
    unnamed x29 -> x33, local copies, waits for them, and re-layouts: 8.72 us -> 1.86 us
    psum x1 -> x0, blocking collectives: 6.31 us -> none  [on_device(): square_sum_q, square_sum_o = lax.psum((square_sum_q, square_sum_o), 'tp')]
    reshape x2 -> x0, local copies, waits for them, and re-layouts: 3.01 us -> none  [the longest x1 2 us: on_device(): piece_output = piece[:, rank:].reshape(2 * count, rank)]
    div x2 -> x0, other arithmetic: 2.96 us -> none  [moments(): return (mean_new, square_new, mean_new / jnp.sqrt(square_new))]
  transfers between devices with their start and end apart: 2 -> 0, of which waited for: 2 -> 0; matrix products, arithmetic and copies ran while one was open for 2% -> 0% of each run, Pallas kernels for 0% -> 0%
where the time goes in v1:
time: 71.8 us; the launch traced here: 71.6 us
  Pallas kernels  59.4 us (83%)
  matrix products  5.47 us (8%)
  local copies, waits for them, and re-layouts  3.22 us (4%)
  between operations  2.23 us (3%)
  other arithmetic  1.33 us (2%)
    pallas_call x1, Pallas kernels, on_device(): pl.pallas_call(functools.partial(fused_kernel, nz, ny, nt, inv_root), nam...  59.4 us
    dot_general x2, matrix products, finish(): step = jnp.dot(factor, direction, preferred_element_type=F32) * scale  2.99 us
    dot_general x2, matrix products, finish(): jnp.dot(factor_all.reshape(-1, rank), direction, preferred_element_type=F32)  2.49 us
    unnamed x33, local copies, waits for them, and re-layouts  1.86 us

profile of v1, /device:TPU:0, one launch (start us, length us, event | category | flops | bytes accessed | tf_op | source)
XLA Modules:
  0.0 71.6 jit_solution(9306773971095887273)
XLA Ops:
  0.6 0.0 copy-start.2
  0.7 0.0 copy-start
  0.7 0.0 copy-start.10
  0.7 0.0 copy-start.3
  0.7 59.4 %moment_exchange.1 = (bf16[4,2,192,256]{3,2,1,0:T(8,128)(2,1)}, bf16[4,2,64,384]{3,2,1,0:T(8,128)(2,1)}, bf16[4,2,128,512]{3,2,1,0:T(8,128)(2,1)}, bf16[4,2,32,3...) custom-call(bf16[3072,512]{1,0:T(8,128)(2,1)} %latent_hbm.1, ...), custom_call_target="tpu_custom_call" | custom-call | tf_op jit(solution)/shard_map/moment_exchange/pallas_call | solution.py:282
  60.1 0.0 copy-start.1
  60.1 0.0 copy-start.7
  60.1 0.0 copy-start.14
  60.1 1.3 %fusion.8 = (f32[1,1,1]{2,1,0:T(1,128)}, f32[1,1,1]{2,1,0:T(1,128)}) fusion(f32[2,8,128]{2,1,0:T(8,128)} %get-tuple-element.19), kind=kLoop, calls=%fused_computation.18 | loop fusion | bytes 16 | tf_op jit(solution)/shard_map/slice | solution.py:333
  62.1 0.0 copy-done.2
  62.1 0.0 copy-done.10
  62.1 1.8 %multiply_subtract_fusion.1 = (f32[64,384]{1,0:T(8,128)}, f32[64,384]{1,0:T(8,128)}) fusion(f32[64,384]{1,0:T(8,128)S(1)} %copy-done.2, f32[]{:T(128)} %bitcast.1, bf16[64,256]{1,0:T(8,128)(2,1)S(1)} %copy-done.10, bf16[256,384]{1,0:T(8,128)(2,1)} %bitcast.26), kind=kOutput, calls=%fused_computation.12 | convolution fusion | flops 12656640 | bytes 524292 | tf_op jit(solution)/shard_map/dot_general | solution.py:335
  63.9 0.0 copy-done
  63.9 0.1 copy.22
  64.7 0.0 copy-done.3
  64.7 1.2 %multiply_subtract_fusion = (f32[128,512]{0,1:T(8,128)S(1)}, f32[128,512]{0,1:T(8,128)S(1)}) fusion(f32[128,512]{0,1:T(8,128)S(1)} %copy.22, f32[]{:T(128)} %bitcast.4, bf16[256,512]{1,0:T(8,128)(2,1)} %bitcast.24, bf16[128,256]{1,0:T(8,128)(2,1)S(1)} %copy-done.3), kind=kOutput, calls=%fused_computation.10 | convolution fusion | flops 33751040 | bytes 1114116 | tf_op jit(solution)/shard_map/dot_general | solution.py:335
  65.9 0.0 copy-start.6
  66.0 0.0 copy-start.13
  66.0 0.8 %copy.23 = f32[128,512]{1,0:T(8,128)} copy(f32[128,512]{0,1:T(8,128)S(1)} %get-tuple-element.45) | data formatting | bytes 524288
  66.8 0.8 %copy.24 = f32[128,512]{1,0:T(8,128)} copy(f32[128,512]{0,1:T(8,128)S(1)} %get-tuple-element.44) | data formatting | bytes 524288
  67.6 0.0 copy-done.1
  67.7 0.0 copy-done.7
  67.7 0.0 copy-done.14
  67.7 1.0 %fusion.3 = bf16[512,384]{1,0:T(8,128)(2,1)} fusion(bf16[512,256]{1,0:T(8,128)(2,1)S(1)} %bitcast.23, bf16[256,384]{1,0:T(8,128)(2,1)S(1)} %bitcast.27, bf16[512,384]{1,0:T(8,128)(2,1)S(1)} %bitcast.29, f32[]{:T(128)} %bitcast.1), kind=kOutput, calls=%fused_computation.5 | convolution fusion | flops 101646336 | bytes 1245188 | tf_op jit(solution)/shard_map/dot_general | solution.py:337
  68.7 0.0 copy-start.5
  68.7 0.0 copy-start.11
  68.8 1.4 %fusion = bf16[1024,512]{1,0:T(8,128)(2,1)} fusion(bf16[1024,512]{1,0:T(8,128)(2,1)S(1)} %bitcast.28, bf16[1024,256]{1,0:T(8,128)(2,1)S(1)} %bitcast.22, bf16[256,512]{1,0:T(8,128)(2,1)S(1)} %bitcast.25, f32[]{:T(128)} %bitcast.4), kind=kOutput, calls=%fused_computation.1 | convolution fusion | flops 271056896 | bytes 2883588 | tf_op jit(solution)/shard_map/dot_general | solution.py:337
  70.3 0.0 copy-done.8
  70.3 0.7 fusion.7
  70.9 0.0 copy-done.4
  70.9 0.0 copy-done.11
  70.9 0.7 fusion.6
  (11 shorter events, 0.1 us)
Async XLA Ops:
  0.6 61.4 %copy-start.2 = (f32[64,384]{1,0:T(8,128)S(1)}, f32[64,384]{1,0:T(8,128)}, u32[]{:S(2)}) copy-start(f32[64,384]{1,0:T(8,128)} %wq_ref.1) | copy-start | bytes 294916
  0.7 63.2 %copy-start = (f32[128,512]{1,0:T(8,128)S(1)}, f32[128,512]{1,0:T(8,128)}, u32[]{:S(2)}) copy-start(f32[128,512]{1,0:T(8,128)} %wo_ref.1) | copy-start | bytes 786436
  0.7 61.4 %copy-start.10 = (bf16[64,256]{1,0:T(8,128)(2,1)S(1)}, bf16[64,256]{1,0:T(8,128)(2,1)}, u32[]{:S(2)}) copy-start(bf16[64,256]{1,0:T(8,128)(2,1)} %fq_hbm.1) | copy-start | bytes 98308
  0.7 64.0 %copy-start.3 = (bf16[128,256]{1,0:T(8,128)(2,1)S(1)}, bf16[128,256]{1,0:T(8,128)(2,1)}, u32[]{:S(2)}) copy-start(bf16[128,256]{1,0:T(8,128)(2,1)} %fo_hbm.1) | copy-start | bytes 196612
  60.1 7.6 %copy-start.1 = (bf16[4,2,192,256]{3,2,1,0:T(8,128)(2,1)S(1)}, bf16[4,2,192,256]{3,2,1,0:T(8,128)(2,1)}, u32[]{:S(2)}) copy-start(bf16[4,2,192,256]{3,2,1,0:T(8,128)(2,1)} %get-tuple-element.22) | copy-start | bytes 2359300
  60.1 7.6 %copy-start.7 = (bf16[4,2,32,384]{3,2,1,0:T(8,128)(2,1)S(1)}, bf16[4,2,32,384]{3,2,1,0:T(8,128)(2,1)}, u32[]{:S(2)}) copy-start(bf16[4,2,32,384]{3,2,1,0:T(8,128)(2,1)} %get-tuple-element.18) | copy-start | bytes 589828
  60.1 7.6 %copy-start.14 = (bf16[4,2,64,384]{3,2,1,0:T(8,128)(2,1)S(1)}, bf16[4,2,64,384]{3,2,1,0:T(8,128)(2,1)}, u32[]{:S(2)}) copy-start(bf16[4,2,64,384]{3,2,1,0:T(8,128)(2,1)} %get-tuple-element.21) | copy-start | bytes 1179652
  65.9 2.9 %copy-start.6 = (bf16[4,2,32,512]{3,2,1,0:T(8,128)(2,1)S(1)}, bf16[4,2,32,512]{3,2,1,0:T(8,128)(2,1)}, u32[]{:S(2)}) copy-start(bf16[4,2,32,512]{3,2,1,0:T(8,128)(2,1)} %get-tuple-element.20) | copy-start | bytes 786436
  66.0 2.9 %copy-start.13 = (bf16[4,2,128,512]{3,2,1,0:T(8,128)(2,1)S(1)}, bf16[4,2,128,512]{3,2,1,0:T(8,128)(2,1)}, u32[]{:S(2)}) copy-start(bf16[4,2,128,512]{3,2,1,0:T(8,128)(2,1)} %get-tuple-element.23) | copy-start | bytes 3145732
  68.7 1.5 %copy-start.8 = (f32[32,384]{1,0:T(8,128)S(1)}, f32[32,384]{1,0:T(8,128)}, u32[]{:S(2)}) copy-start(f32[32,384]{1,0:T(8,128)} %qm_ref.1) | copy-start | bytes 147460
  68.7 1.5 %copy-start.9 = (f32[32,384]{1,0:T(8,128)S(1)}, f32[32,384]{1,0:T(8,128)}, u32[]{:S(2)}) copy-start(f32[32,384]{1,0:T(8,128)} %qs_ref.1) | copy-start | bytes 147460
  68.7 1.5 %copy-start.12 = (f32[32,384]{1,0:T(8,128)S(1)}, f32[32,384]{1,0:T(8,128)}, u32[]{:S(2)}) copy-start(f32[32,384]{1,0:T(8,128)} %get-tuple-element.24) | copy-start | bytes 147460
  68.7 2.2 %copy-start.4 = (f32[32,512]{1,0:T(8,128)S(1)}, f32[32,512]{1,0:T(8,128)}, u32[]{:S(2)}) copy-start(f32[32,512]{1,0:T(8,128)} %om_ref.1) | copy-start | bytes 196612
  68.7 2.2 %copy-start.5 = (f32[32,512]{1,0:T(8,128)S(1)}, f32[32,512]{1,0:T(8,128)}, u32[]{:S(2)}) copy-start(f32[32,512]{1,0:T(8,128)} %os_ref.1) | copy-start | bytes 196612
  68.7 2.2 %copy-start.11 = (f32[32,512]{1,0:T(8,128)S(1)}, f32[32,512]{1,0:T(8,128)}, u32[]{:S(2)}) copy-start(f32[32,512]{1,0:T(8,128)} %get-tuple-element.25) | copy-start | bytes 196612

commit v2 on v1

--- a/solution.py
+++ b/solution.py
@@ -124,6 +124,7 @@
     w_z = {}
     for d in early:
         w_z[d] = (send(wo_block(z), wo_block(z), to_z(d)), send(wq_block(z), wq_block(z), to_z(d)))
+    w_y = y_send(wo_block, 0) + y_send(wq_block, 0)
 
     grad_o[...] = jnp.zeros_like(grad_o)
     grad_q[...] = jnp.zeros_like(grad_q)
@@ -210,7 +211,6 @@
     for d in far:
         if d not in w_z:
             w_z[d] = (send(wo_block(z), wo_block(z), to_z(d)), send(wq_block(z), wq_block(z), to_z(d)))
-    w_y = y_send(wo_block, 0) + y_send(wq_block, 0)
 
     def forward_weights(d):
         w_z[d][0].wait_recv()

time: 71.8 us -> 71.8 us (level)
  no operation moved by 1% of the time
where the time goes in v2:
time: 71.8 us; the launch traced here: 71.6 us
  Pallas kernels  59.4 us (83%)
  matrix products  5.47 us (8%)
  local copies, waits for them, and re-layouts  3.22 us (4%)
  between operations  2.23 us (3%)
  other arithmetic  1.33 us (2%)
    pallas_call x1, Pallas kernels, on_device(): pl.pallas_call(functools.partial(fused_kernel, nz, ny, nt, inv_root), nam...  59.4 us
    dot_general x2, matrix products, finish(): step = jnp.dot(factor, direction, preferred_element_type=F32) * scale  2.99 us
    dot_general x2, matrix products, finish(): jnp.dot(factor_all.reshape(-1, rank), direction, preferred_element_type=F32)  2.49 us
    unnamed x33, local copies, waits for them, and re-layouts  1.86 us

profile of v2, /device:TPU:0, one launch (start us, length us, event | category | flops | bytes accessed | tf_op | source)
XLA Modules:
  0.0 71.6 jit_solution(4133091796622486584)
XLA Ops:
  0.6 0.0 copy-start.2
  0.7 0.0 copy-start
  0.7 0.0 copy-start.10
  0.7 0.0 copy-start.3
  0.7 59.4 %moment_exchange.1 = (bf16[4,2,192,256]{3,2,1,0:T(8,128)(2,1)}, bf16[4,2,64,384]{3,2,1,0:T(8,128)(2,1)}, bf16[4,2,128,512]{3,2,1,0:T(8,128)(2,1)}, bf16[4,2,32,3...) custom-call(bf16[3072,512]{1,0:T(8,128)(2,1)} %latent_hbm.1, ...), custom_call_target="tpu_custom_call" | custom-call | tf_op jit(solution)/shard_map/moment_exchange/pallas_call | solution.py:282
  60.1 0.0 copy-start.1
  60.1 0.0 copy-start.7
  60.1 0.0 copy-start.14
  60.1 1.3 %fusion.8 = (f32[1,1,1]{2,1,0:T(1,128)}, f32[1,1,1]{2,1,0:T(1,128)}) fusion(f32[2,8,128]{2,1,0:T(8,128)} %get-tuple-element.19), kind=kLoop, calls=%fused_computation.18 | loop fusion | bytes 16 | tf_op jit(solution)/shard_map/slice | solution.py:333
  62.1 0.0 copy-done.2
  62.1 0.0 copy-done.10
  62.1 1.8 %multiply_subtract_fusion.1 = (f32[64,384]{1,0:T(8,128)}, f32[64,384]{1,0:T(8,128)}) fusion(f32[64,384]{1,0:T(8,128)S(1)} %copy-done.2, f32[]{:T(128)} %bitcast.1, bf16[64,256]{1,0:T(8,128)(2,1)S(1)} %copy-done.10, bf16[256,384]{1,0:T(8,128)(2,1)} %bitcast.26), kind=kOutput, calls=%fused_computation.12 | convolution fusion | flops 12656640 | bytes 524292 | tf_op jit(solution)/shard_map/dot_general | solution.py:335
  63.9 0.0 copy-done
  63.9 0.1 copy.22
  64.7 0.0 copy-done.3
  64.7 1.2 %multiply_subtract_fusion = (f32[128,512]{0,1:T(8,128)S(1)}, f32[128,512]{0,1:T(8,128)S(1)}) fusion(f32[128,512]{0,1:T(8,128)S(1)} %copy.22, f32[]{:T(128)} %bitcast.4, bf16[256,512]{1,0:T(8,128)(2,1)} %bitcast.24, bf16[128,256]{1,0:T(8,128)(2,1)S(1)} %copy-done.3), kind=kOutput, calls=%fused_computation.10 | convolution fusion | flops 33751040 | bytes 1114116 | tf_op jit(solution)/shard_map/dot_general | solution.py:335
  65.9 0.0 copy-start.6
  66.0 0.0 copy-start.13
  66.0 0.8 %copy.23 = f32[128,512]{1,0:T(8,128)} copy(f32[128,512]{0,1:T(8,128)S(1)} %get-tuple-element.45) | data formatting | bytes 524288
  66.8 0.8 %copy.24 = f32[128,512]{1,0:T(8,128)} copy(f32[128,512]{0,1:T(8,128)S(1)} %get-tuple-element.44) | data formatting | bytes 524288
  67.6 0.0 copy-done.1
  67.7 0.0 copy-done.7
  67.7 0.0 copy-done.14
  67.7 1.0 %fusion.3 = bf16[512,384]{1,0:T(8,128)(2,1)} fusion(bf16[512,256]{1,0:T(8,128)(2,1)S(1)} %bitcast.23, bf16[256,384]{1,0:T(8,128)(2,1)S(1)} %bitcast.27, bf16[512,384]{1,0:T(8,128)(2,1)S(1)} %bitcast.29, f32[]{:T(128)} %bitcast.1), kind=kOutput, calls=%fused_computation.5 | convolution fusion | flops 101646336 | bytes 1245188 | tf_op jit(solution)/shard_map/dot_general | solution.py:337
  68.7 0.0 copy-start.5
  68.7 0.0 copy-start.11
  68.8 0.0 copy-done.6
  68.8 0.0 copy-done.13
  68.8 1.4 %fusion = bf16[1024,512]{1,0:T(8,128)(2,1)} fusion(bf16[1024,512]{1,0:T(8,128)(2,1)S(1)} %bitcast.28, bf16[1024,256]{1,0:T(8,128)(2,1)S(1)} %bitcast.22, bf16[256,512]{1,0:T(8,128)(2,1)S(1)} %bitcast.25, f32[]{:T(128)} %bitcast.4), kind=kOutput, calls=%fused_computation.1 | convolution fusion | flops 271056896 | bytes 2883588 | tf_op jit(solution)/shard_map/dot_general | solution.py:337
  70.3 0.0 copy-done.8
  70.3 0.7 fusion.7
  70.9 0.7 fusion.6
  (11 shorter events, 0.1 us)
Async XLA Ops:
  0.6 61.4 %copy-start.2 = (f32[64,384]{1,0:T(8,128)S(1)}, f32[64,384]{1,0:T(8,128)}, u32[]{:S(2)}) copy-start(f32[64,384]{1,0:T(8,128)} %wq_ref.1) | copy-start | bytes 294916
  0.7 63.2 %copy-start = (f32[128,512]{1,0:T(8,128)S(1)}, f32[128,512]{1,0:T(8,128)}, u32[]{:S(2)}) copy-start(f32[128,512]{1,0:T(8,128)} %wo_ref.1) | copy-start | bytes 786436
  0.7 61.4 %copy-start.10 = (bf16[64,256]{1,0:T(8,128)(2,1)S(1)}, bf16[64,256]{1,0:T(8,128)(2,1)}, u32[]{:S(2)}) copy-start(bf16[64,256]{1,0:T(8,128)(2,1)} %fq_hbm.1) | copy-start | bytes 98308
  0.7 64.0 %copy-start.3 = (bf16[128,256]{1,0:T(8,128)(2,1)S(1)}, bf16[128,256]{1,0:T(8,128)(2,1)}, u32[]{:S(2)}) copy-start(bf16[128,256]{1,0:T(8,128)(2,1)} %fo_hbm.1) | copy-start | bytes 196612
  60.1 7.6 %copy-start.1 = (bf16[4,2,192,256]{3,2,1,0:T(8,128)(2,1)S(1)}, bf16[4,2,192,256]{3,2,1,0:T(8,128)(2,1)}, u32[]{:S(2)}) copy-start(bf16[4,2,192,256]{3,2,1,0:T(8,128)(2,1)} %get-tuple-element.22) | copy-start | bytes 2359300
  60.1 7.6 %copy-start.7 = (bf16[4,2,32,384]{3,2,1,0:T(8,128)(2,1)S(1)}, bf16[4,2,32,384]{3,2,1,0:T(8,128)(2,1)}, u32[]{:S(2)}) copy-start(bf16[4,2,32,384]{3,2,1,0:T(8,128)(2,1)} %get-tuple-element.18) | copy-start | bytes 589828
  60.1 7.6 %copy-start.14 = (bf16[4,2,64,384]{3,2,1,0:T(8,128)(2,1)S(1)}, bf16[4,2,64,384]{3,2,1,0:T(8,128)(2,1)}, u32[]{:S(2)}) copy-start(bf16[4,2,64,384]{3,2,1,0:T(8,128)(2,1)} %get-tuple-element.21) | copy-start | bytes 1179652
  65.9 2.9 %copy-start.6 = (bf16[4,2,32,512]{3,2,1,0:T(8,128)(2,1)S(1)}, bf16[4,2,32,512]{3,2,1,0:T(8,128)(2,1)}, u32[]{:S(2)}) copy-start(bf16[4,2,32,512]{3,2,1,0:T(8,128)(2,1)} %get-tuple-element.20) | copy-start | bytes 786436
  66.0 2.9 %copy-start.13 = (bf16[4,2,128,512]{3,2,1,0:T(8,128)(2,1)S(1)}, bf16[4,2,128,512]{3,2,1,0:T(8,128)(2,1)}, u32[]{:S(2)}) copy-start(bf16[4,2,128,512]{3,2,1,0:T(8,128)(2,1)} %get-tuple-element.23) | copy-start | bytes 3145732
  68.7 1.5 %copy-start.8 = (f32[32,384]{1,0:T(8,128)S(1)}, f32[32,384]{1,0:T(8,128)}, u32[]{:S(2)}) copy-start(f32[32,384]{1,0:T(8,128)} %qm_ref.1) | copy-start | bytes 147460
  68.7 1.5 %copy-start.9 = (f32[32,384]{1,0:T(8,128)S(1)}, f32[32,384]{1,0:T(8,128)}, u32[]{:S(2)}) copy-start(f32[32,384]{1,0:T(8,128)} %qs_ref.1) | copy-start | bytes 147460
  68.7 1.5 %copy-start.12 = (f32[32,384]{1,0:T(8,128)S(1)}, f32[32,384]{1,0:T(8,128)}, u32[]{:S(2)}) copy-start(f32[32,384]{1,0:T(8,128)} %get-tuple-element.24) | copy-start | bytes 147460
  68.7 2.2 %copy-start.4 = (f32[32,512]{1,0:T(8,128)S(1)}, f32[32,512]{1,0:T(8,128)}, u32[]{:S(2)}) copy-start(f32[32,512]{1,0:T(8,128)} %om_ref.1) | copy-start | bytes 196612
  68.7 2.2 %copy-start.5 = (f32[32,512]{1,0:T(8,128)S(1)}, f32[32,512]{1,0:T(8,128)}, u32[]{:S(2)}) copy-start(f32[32,512]{1,0:T(8,128)} %os_ref.1) | copy-start | bytes 196612
  68.7 2.2 %copy-start.11 = (f32[32,512]{1,0:T(8,128)S(1)}, f32[32,512]{1,0:T(8,128)}, u32[]{:S(2)}) copy-start(f32[32,512]{1,0:T(8,128)} %get-tuple-element.25) | copy-start | bytes 196612
